TPU v7x, 32 devices: a whole 2x2x4 slice. The times are simulated.
32 devices in a mesh: rep: 2 (over x), fs: 4 (over y, core), tp: 4 (over z).
Axes of the slice: x: 2, y: 2, z: 4, core: 2. Of those that a mesh axis runs over, the one named last changes fastest.
Arguments:
- tokens: bfloat16 [4096, 2048], P(('rep', 'fs', 'tp')), may hold values from -3 to 3
- mixer_output: bfloat16 [4096, 2048], P(('rep', 'fs', 'tp')), may hold values from -6 to 6
- early_norm: float32 [2048], replicated, may hold values from 0.75 to 1.25
- early_gate: bfloat16 [2048, 5120], P('fs', 'tp'), may hold values from -0.125 to 0.125
- early_value: bfloat16 [2048, 5120], P('fs', 'tp'), may hold values from -0.125 to 0.125
- early_down: bfloat16 [5120, 2048], P('tp', 'fs'), may hold values from -0.078125 to 0.078125
- early_post: float32 [2048], replicated, may hold values from 0.75 to 1.25
- mixer_gain: float32 [2048], replicated, may hold values from 0.75 to 1.25
- later_norm: float32 [2048], replicated, may hold values from 0.75 to 1.25
- later_gate: bfloat16 [2048, 5120], P('fs', 'tp'), may hold values from -0.125 to 0.125
- later_value: bfloat16 [2048, 5120], P('fs', 'tp'), may hold values from -0.125 to 0.125
- later_down: bfloat16 [5120, 2048], P('tp', 'fs'), may hold values from -0.078125 to 0.078125
- later_post: float32 [2048], replicated, may hold values from 0.75 to 1.25
Outputs:
- layer_out: bfloat16 [4096, 2048], P(('rep', 'fs', 'tp'))
All inputs are finite; a program needn't handle non-finite values.
Results may differ from a plain program's by a relative error of at most 0.015.
Values may be sent and summed in bfloat16 or wider, within the bound.
A program may use at most 128 MiB of HBM per device.

v0:
```python
import jax
import jax.numpy as jnp
from jax import lax
from jax.sharding import PartitionSpec as P

epsilon = 1e-06


def over_all(piece, axis, dim, step, start):
    def gathered(part):
        return lax.all_gather(part, axis, axis=dim, tiled=True)

    return step(start, jax.tree.map(gathered, piece), jnp.int32(0))


def own_rows(product, extent, axis):
    everything = product(jnp.int32(0), lax.axis_size(axis) * extent)
    own = lax.psum_scatter(everything.astype(jnp.bfloat16), axis, scatter_dimension=0, tiled=True)
    return own.astype(jnp.float32)


def rms_scale(values, gain):
    values = values.astype(jnp.float32)
    scale = lax.rsqrt(jnp.mean(values * values, axis=-1, keepdims=True) + epsilon)
    return values * scale * gain


def half_branch(normed, gate_piece, value_piece, down_piece):
    all_rows = lax.all_gather(normed, "tp", axis=0, tiled=True)
    empty = jnp.zeros((all_rows.shape[0], gate_piece.shape[1]), jnp.float32)

    def add_rows(totals, pieces, start):
        columns = lax.dynamic_slice_in_dim(all_rows, start, pieces[0].shape[0], 1)
        gate_part = jnp.dot(columns, pieces[0], preferred_element_type=jnp.float32)
        value_part = jnp.dot(columns, pieces[1], preferred_element_type=jnp.float32)
        return (totals[0] + gate_part, totals[1] + value_part)

    gate_sum, value_sum = over_all((gate_piece, value_piece), "fs", 0, add_rows, (empty, empty))
    down_block = lax.all_gather(down_piece, "fs", axis=1, tiled=True)
    hidden = (jax.nn.silu(gate_sum) * value_sum).astype(jnp.bfloat16)

    def row_term(start, count):
        rows = lax.dynamic_slice_in_dim(hidden, start, count, 0)
        return jnp.dot(rows, down_block, preferred_element_type=jnp.float32)

    return own_rows(row_term, normed.shape[0], "tp")


def on_device(
    tokens,
    mixer_output,
    early_norm,
    early_gate,
    early_value,
    early_down,
    early_post,
    mixer_gain,
    later_norm,
    later_gate,
    later_value,
    later_down,
    later_post,
):
    early_in = rms_scale(tokens, early_norm).astype(jnp.bfloat16)
    early_branch = half_branch(early_in, early_gate, early_value, early_down)
    mixed = (
        tokens.astype(jnp.float32)
        + 0.5 * rms_scale(early_branch, early_post)
        + rms_scale(mixer_output, mixer_gain)
    )
    mixed = mixed.astype(jnp.bfloat16)
    later_in = rms_scale(mixed, later_norm).astype(jnp.bfloat16)
    later_branch = half_branch(later_in, later_gate, later_value, later_down)
    layer_out = mixed.astype(jnp.float32) + 0.5 * rms_scale(later_branch, later_post)
    return layer_out.astype(jnp.bfloat16)


def solution(mesh):
    placed = (
        P(("rep", "fs", "tp"), None),
        P(("rep", "fs", "tp"), None),
        P(),
        P("fs", "tp"),
        P("fs", "tp"),
        P("tp", "fs"),
        P(),
        P(),
        P(),
        P("fs", "tp"),
        P("fs", "tp"),
        P("tp", "fs"),
        P(),
    )
    return jax.shard_map(
        on_device,
        mesh=mesh,
        in_specs=placed,
        out_specs=P(("rep", "fs", "tp"), None),
        check_vma=False,
    )
```

profile of v0, /device:TPU:0, one launch (start us, length us, event | category | flops | bytes accessed | tf_op | source)
XLA Modules:
  0.0 476.7 jit_solution(1629845041237749501)
XLA Ops:
  6.5 1.2 fusion.12
  7.8 2.0 fusion.14
  9.9 0.7 all-gather.11.cloned.1.call-update
  10.6 0.7 all-gather.13.cloned.1.call-update
  11.4 0.5 all-gather.15.cloned.1.call-update
  11.9 46.2 %all-gather.9.cloned.1.call-done = bf16[512,2048]{1,0:T(8,128)(2,1)} async-done(((bf16[128,2048]{1,0:T(8,128)(2,1)}), bf16[512,2048]{1,0:T(8,128)(2,1)}) %all-gather.9.cloned.1.call-update) | async-done | bytes 2097168 | tf_op jit(solution)/shard_map/all_gather | solution.py:29
  58.2 40.9 %all-gather.11.cloned.1.call-done = bf16[2048,1280]{1,0:T(8,128)(2,1)} async-done(((bf16[512,1280]{1,0:T(8,128)(2,1)}), bf16[2048,1280]{1,0:T(8,128)(2,1)}) %all-gather.11.cloned.1.call-update) | async-done | bytes 5242896 | tf_op jit(solution)/shard_map/all_gather | solution.py:11
  99.1 7.5 %fusion.22 = f32[512,1280]{1,0:T(8,128)} fusion(bf16[512,2048]{1,0:T(8,128)(2,1)} %all-gather.9.cloned.1.call-done, bf16[2048,1280]{1,0:T(8,128)(2,1)} %all-gather.11.cloned.1.call-done), kind=kOutput, calls=%fused_computation.42 | convolution fusion | flops 2684354560 | bytes 9961472 | tf_op jit(solution)/shard_map/dot_general | solution.py:34
  106.6 34.4 %all-gather.13.cloned.1.call-done = bf16[2048,1280]{1,0:T(8,128)(2,1)} async-done(((bf16[512,1280]{1,0:T(8,128)(2,1)}), bf16[2048,1280]{1,0:T(8,128)(2,1)}) %all-gather.13.cloned.1.call-update) | async-done | bytes 5242896 | tf_op jit(solution)/shard_map/all_gather | solution.py:11
  141.0 41.8 %all-gather.15.cloned.1.call-done = bf16[1280,2048]{1,0:T(8,128)(2,1)} async-done(((bf16[1280,512]{1,0:T(8,128)(2,1)}), bf16[1280,2048]{1,0:T(8,128)(2,1)}) %all-gather.15.cloned.1.call-update) | async-done | bytes 5242896 | tf_op jit(solution)/shard_map/all_gather | solution.py:39
  182.7 12.5 %convolution_convert_fusion.1 = bf16[512,2048]{1,0:T(8,128)(2,1)} fusion(bf16[1280,2048]{1,0:T(8,128)(2,1)} %all-gather.15.cloned.1.call-done, bf16[512,2048]{1,0:T(8,128)(2,1)S(1)} %copy-done.6, bf16[2048,1280]{1,0:T(8,128)(2,1)} %all-gather.13.cloned.1.call-done, f32[512,1280]{1,0:T(8,128)} %fusion.22), kind=kOutput, calls=%fused_computation.5 | convolution fusion | flops 5373689856 | bytes 17301504 | tf_op jit(solution)/shard_map/dot_general | solution.py:44
  195.3 0.0 all-gather.19.cloned.1.call-start
  195.3 0.5 all-gather.19.cloned.1.call-update
  195.9 0.4 copy-done.1
  196.3 0.2 fusion.5
  196.4 42.9 %reduce-scatter.3.cloned.1.call-done = bf16[128,2048]{1,0:T(8,128)(2,1)} async-done(((bf16[512,2048]{1,0:T(8,128)(2,1)}), bf16[128,2048]{1,0:T(8,128)(2,1)}) %reduce-scatter.3.cloned.1.call-update) | async-done | bytes 524304 | tf_op jit(solution)/shard_map/reduce_scatter | solution.py:18
  239.3 1.2 fusion.2
  240.6 1.6 fusion.15
  242.2 1.0 fusion.17
  243.3 0.0 all-gather.21.cloned.1.call-start
  243.3 0.7 all-gather.21.cloned.1.call-update
  244.1 0.7 all-gather.23.cloned.1.call-update
  244.7 0.2 reduce-scatter.5.cloned.1.call-start
  245.0 35.1 %all-gather.19.cloned.1.call-done = bf16[2048,1280]{1,0:T(8,128)(2,1)} async-done(((bf16[512,1280]{1,0:T(8,128)(2,1)}), bf16[2048,1280]{1,0:T(8,128)(2,1)}) %all-gather.19.cloned.1.call-update) | async-done | bytes 5242896 | tf_op jit(solution)/shard_map/all_gather | solution.py:11
  280.0 47.0 %all-gather.17.cloned.1.call-done = bf16[512,2048]{1,0:T(8,128)(2,1)} async-done(((bf16[128,2048]{1,0:T(8,128)(2,1)}), bf16[512,2048]{1,0:T(8,128)(2,1)}) %all-gather.17.cloned.1.call-update) | async-done | bytes 2097168 | tf_op jit(solution)/shard_map/all_gather | solution.py:29
  327.1 7.6 %fusion.23 = f32[512,1280]{1,0:T(8,128)} fusion(bf16[512,2048]{1,0:T(8,128)(2,1)} %all-gather.17.cloned.1.call-done, bf16[2048,1280]{1,0:T(8,128)(2,1)} %all-gather.19.cloned.1.call-done), kind=kOutput, calls=%fused_computation.43 | convolution fusion | flops 2684354560 | bytes 9961472 | tf_op jit(solution)/shard_map/dot_general | solution.py:34
  334.7 33.3 %all-gather.21.cloned.1.call-done = bf16[2048,1280]{1,0:T(8,128)(2,1)} async-done(((bf16[512,1280]{1,0:T(8,128)(2,1)}), bf16[2048,1280]{1,0:T(8,128)(2,1)}) %all-gather.21.cloned.1.call-update) | async-done | bytes 5242896 | tf_op jit(solution)/shard_map/all_gather | solution.py:11
  368.0 41.9 %all-gather.23.cloned.1.call-done = bf16[1280,2048]{1,0:T(8,128)(2,1)} async-done(((bf16[1280,512]{1,0:T(8,128)(2,1)}), bf16[1280,2048]{1,0:T(8,128)(2,1)}) %all-gather.23.cloned.1.call-update) | async-done | bytes 5242896 | tf_op jit(solution)/shard_map/all_gather | solution.py:39
  409.9 12.5 %convolution_convert_fusion = bf16[512,2048]{1,0:T(8,128)(2,1)} fusion(bf16[1280,2048]{1,0:T(8,128)(2,1)} %all-gather.23.cloned.1.call-done, bf16[512,2048]{1,0:T(8,128)(2,1)S(1)} %copy-done.7, bf16[2048,1280]{1,0:T(8,128)(2,1)} %all-gather.21.cloned.1.call-done, f32[512,1280]{1,0:T(8,128)} %fusion.23), kind=kOutput, calls=%fused_computation.4 | convolution fusion | flops 5373689856 | bytes 17301504 | tf_op jit(solution)/shard_map/dot_general | solution.py:44
  422.4 44.1 %reduce-scatter.5.cloned.1.call-done = bf16[128,2048]{1,0:T(8,128)(2,1)} async-done(((bf16[512,2048]{1,0:T(8,128)(2,1)}), bf16[128,2048]{1,0:T(8,128)(2,1)}) %reduce-scatter.5.cloned.1.call-update) | async-done | bytes 524304 | tf_op jit(solution)/shard_map/reduce_scatter | solution.py:18
  466.5 1.2 fusion.9
  467.7 2.1 fusion.18
  (31 shorter events, 0.4 us)
Async XLA Ops:
  6.5 51.6 %all-gather.9.cloned.1.call-start = ((), (), s32[]{:S(2)}) async-start(), calls=%async_computation.2 | async-start | bytes 2621440 | tf_op jit(solution)/shard_map/all_gather | solution.py:29
  9.8 89.2 %all-gather.11.cloned.1.call-start = ((), (), s32[]{:S(2)}) async-start(), calls=%async_computation.3 | async-start | bytes 6553600 | tf_op jit(solution)/shard_map/all_gather | solution.py:11
  10.6 130.4 %all-gather.13.cloned.1.call-start = ((), (), s32[]{:S(2)}) async-start(), calls=%async_computation.4 | async-start | bytes 6553600 | tf_op jit(solution)/shard_map/all_gather | solution.py:11
  11.3 171.4 %all-gather.15.cloned.1.call-start = ((), (), s32[]{:S(2)}) async-start(), calls=%async_computation.5 | async-start | bytes 6553600 | tf_op jit(solution)/shard_map/all_gather | solution.py:39
  11.9 227.5 %reduce-scatter.3.cloned.1.call-start = ((), (), s32[]{:S(2)}) async-start(), calls=%async_computation.6 | async-start | bytes 2621440 | tf_op jit(solution)/shard_map/reduce_scatter | solution.py:18
  58.2 124.6 %copy-start.6 = (bf16[512,2048]{1,0:T(8,128)(2,1)S(1)}, bf16[512,2048]{1,0:T(8,128)(2,1)}, u32[]{:S(2)}) copy-start(bf16[512,2048]{1,0:T(8,128)(2,1)} %all-gather.9.cloned.1.call-done) | copy-start | bytes 6291460
  195.2 1.0 copy-start.1
  195.2 45.4 %copy-start = (bf16[128,2048]{1,0:T(8,128)(2,1)S(1)}, bf16[128,2048]{1,0:T(8,128)(2,1)}, u32[]{:S(2)}) copy-start(bf16[128,2048]{1,0:T(8,128)(2,1)} %param.13) | copy-start | bytes 1572868
  195.2 45.4 %copy-start.2 = (f32[2048]{0:T(1024)S(1)}, f32[2048]{0:T(1024)}, u32[]{:S(2)}) copy-start(f32[2048]{0:T(1024)} %param.20) | copy-start | bytes 24580
  195.2 45.4 %copy-start.3 = (f32[2048]{0:T(1024)S(1)}, f32[2048]{0:T(1024)}, u32[]{:S(2)}) copy-start(f32[2048]{0:T(1024)} %param.19) | copy-start | bytes 24580
  195.2 47.0 %copy-start.4 = (f32[2048]{0:T(1024)S(1)}, f32[2048]{0:T(1024)}, u32[]{:S(2)}) copy-start(f32[2048]{0:T(1024)} %param.21) | copy-start | bytes 24580
  195.3 84.8 %all-gather.19.cloned.1.call-start = ((), (), s32[]{:S(2)}) async-start(), calls=%async_computation.8 | async-start | bytes 6553600 | tf_op jit(solution)/shard_map/all_gather | solution.py:11
  195.8 131.2 %all-gather.17.cloned.1.call-start = ((), (), s32[]{:S(2)}) async-start(), calls=%async_computation.7 | async-start | bytes 2621440 | tf_op jit(solution)/shard_map/all_gather | solution.py:29
  243.3 124.7 %all-gather.21.cloned.1.call-start = ((), (), s32[]{:S(2)}) async-start(), calls=%async_computation.9 | async-start | bytes 6553600 | tf_op jit(solution)/shard_map/all_gather | solution.py:11
  244.0 165.9 %all-gather.23.cloned.1.call-start = ((), (), s32[]{:S(2)}) async-start(), calls=%async_computation.10 | async-start | bytes 6553600 | tf_op jit(solution)/shard_map/all_gather | solution.py:39
  244.7 221.8 %reduce-scatter.5.cloned.1.call-start = ((), (), s32[]{:S(2)}) async-start(), calls=%async_computation.11 | async-start | bytes 2621440 | tf_op jit(solution)/shard_map/reduce_scatter | solution.py:18
  327.1 82.8 %copy-start.7 = (bf16[512,2048]{1,0:T(8,128)(2,1)S(1)}, bf16[512,2048]{1,0:T(8,128)(2,1)}, u32[]{:S(2)}) copy-start(bf16[512,2048]{1,0:T(8,128)(2,1)} %all-gather.17.cloned.1.call-done) | copy-start | bytes 6291460
  422.4 45.4 %copy-start.5 = (f32[2048]{0:T(1024)S(1)}, f32[2048]{0:T(1024)}, u32[]{:S(2)}) copy-start(f32[2048]{0:T(1024)} %param.25) | copy-start | bytes 24580
Sparse Core Ops, SparseCore 0:
  9.9 48.1 all-gather.8
  59.7 39.3 all-gather.10
  100.6 40.2 all-gather.12
  142.4 40.2 all-gather.14
  195.4 43.9 reduce-scatter.2
  240.8 39.2 all-gather.18
  281.6 45.4 all-gather.16
  328.6 39.3 all-gather.20
  369.5 40.2 all-gather.22
  422.5 43.9 reduce-scatter.4
where the time goes:
time: 477 us
  waiting for transfers between devices  411 us (86%)
  matrix products  40.1 us (8%)
  between operations  13.6 us (3%)
  other arithmetic  10.7 us (2%)
    all_gather x4, waiting for transfers between devices, gathered(): return lax.all_gather(part, axis, axis=dim, tiled=True)  144 us
    all_gather x2, waiting for transfers between devices, half_branch(): all_rows = lax.all_gather(normed, 'tp', axis=0, tiled=True)  93.2 us
    reduce_scatter x2, waiting for transfers between devices, own_rows(): lax.psum_scatter(everything.astype(jnp.bfloat16), axis, scatter_dimension...  87 us
    all_gather x2, waiting for transfers between devices, half_branch(): down_block = lax.all_gather(down_piece, 'fs', axis=1, tiled=True)  83.7 us
    dot_general x2, matrix products, row_term(): return jnp.dot(rows, down_block, preferred_element_type=jnp.float32)  25 us
    dot_general x2, matrix products, add_rows(): gate_part = jnp.dot(columns, pieces[0], preferred_element_type=jnp.float32)  15.1 us
  transfers between devices with their start and end apart: 10, of which 10 were waited for; matrix products, arithmetic and copies ran while one was open for 4% of the time, Pallas kernels for 0%

commit v1 on v0

v1 whole, which is shorter than its diff:
```python
import functools

import jax
import jax.numpy as jnp
from jax import lax
from jax.experimental import pallas as pl
from jax.experimental.pallas import tpu as pltpu
from jax.sharding import PartitionSpec as P

epsilon = 1e-06
CORES = 2


def rms_scale(values, gain):
    scale = lax.rsqrt(jnp.mean(values * values, axis=-1, keepdims=True) + epsilon)
    return values * scale * gain


def kernel(
    R, F, T,
    tokens, mixer, early_norm, w0, w1, w2, early_post, mixer_gain, later_norm, w3, w4, w5, later_post,
    out,
    g0, g1, g2, g3, g4, g5, rows0, rows1, hidden, part, mixed, from_left, from_right,
    w_send, w_recv, local_sem, z_send, z_recv,
):
    source = (w0, w1, w2, w3, w4, w5)
    full = (g0, g1, g2, g3, g4, g5)
    all_rows = (rows0, rows1)
    r, f, t = lax.axis_index("rep"), lax.axis_index("fs"), lax.axis_index("tp")
    G = F // CORES
    g, c = f // CORES, f % CORES
    n, D = tokens.shape
    half = T // 2
    cut = D // 2
    mate = {"fs": g * CORES + 1 - c}
    ahead = {"fs": (g + 1) % G * CORES + c}
    behind = {"fs": (g + G - 1) % G * CORES + c}
    z_right, z_left = {"tp": (t + 1) % T}, {"tp": (t + T - 1) % T}
    peers = [{"rep": (r + k) % R} for k in range(1, R)]

    partners = [mate] + peers
    if G > 1:
        partners += [ahead] if G == 2 else [ahead, behind]
    partners += [z_right] if T == 2 else [z_right, z_left]
    barrier = pltpu.get_barrier_semaphore()
    for who in partners:
        pl.semaphore_signal(barrier, inc=1, device_id=who, device_id_type=pl.DeviceIdType.MESH)
    pl.semaphore_wait(barrier, len(partners))

    pending, done = [], set()

    def send(src, dst, sems, index, who):
        copy = pltpu.make_async_remote_copy(
            src_ref=src, dst_ref=dst, send_sem=sems[0].at[index], recv_sem=sems[1].at[index],
            device_id=who, device_id_type=pl.DeviceIdType.MESH,
        )
        copy.start()
        pending.append(copy)
        return copy

    slots = {}

    def w_index(*key):
        return slots.setdefault(key, len(slots))

    copies = {}

    def piece(m, shard, q):
        if m % 3 == 2:
            count = full[m].shape[1] // R
            return full[m].at[shard, pl.ds(pl.multiple_of(q * count, count), count)]
        depth = source[m].shape[0]
        count = depth // R
        return full[m].at[pl.ds(pl.multiple_of(shard * depth + q * count, count), count)]

    def whole_shard(m, shard):
        if m % 3 == 2:
            return full[m].at[shard]
        depth = source[m].shape[0]
        return full[m].at[pl.ds(pl.multiple_of(shard * depth, depth), depth)]

    W = (w_send, w_recv)

    def w_send_to(key, src, dst, who):
        copies[key] = send(src, dst, W, w_index(*key), who)

    def start_weights(m):
        if G > 1:
            count = source[m].shape[0] // R
            own = source[m].at[pl.ds(pl.multiple_of(r * count, count), count)]
            w_send_to(("ring", m, 1), own, piece(m, f, r), ahead)
        w_send_to(("own", m), source[m], whole_shard(m, f), mate)
        local = pltpu.make_async_copy(source[m], whole_shard(m, f), local_sem.at[m])
        local.start()
        copies["local", m] = local

    def ring_relay(m):
        for s in range(1, G):
            copies["ring", m, s].wait_recv()
            got = piece(m, (g + G - s) % G * CORES + c, r)
            if s < G - 1:
                w_send_to(("ring", m, s + 1), got, got, ahead)
            for k, who in enumerate(peers):
                w_send_to(("peer", m, s, k), got, got, who)
            w_send_to(("mate", m, s), got, got, mate)

    def peer_relay(m):
        for s in range(1, G):
            for k in range(len(peers)):
                copies["peer", m, s, k].wait_recv()
                got = piece(m, (g + G - s) % G * CORES + c, (r + R - 1 - k) % R)
                w_send_to(("pass", m, s, k), got, got, mate)

    def ready(m):
        copies["local", m].wait()
        copies["own", m].wait_recv()
        for s in range(1, G):
            copies["mate", m, s].wait_recv()
            for k in range(len(peers)):
                copies["pass", m, s, k].wait_recv()

    Z = (z_send, z_recv)

    def block(where, ref):
        return ref.at[pl.ds(pl.multiple_of(where * n, n), n)]

    def sides(ref, d):
        return (ref.at[:, :cut], ref.at[:, cut:]) if d == half else (ref, ref)

    def z_slot(phase, layer, step, way):
        return ((phase * 2 + layer) * half + step) * 2 + way

    def gather_send(layer, d):
        rows = all_rows[layer]
        a = sides(block((t + T - (d - 1)) % T, rows), d)[0]
        b = sides(block((t + d - 1) % T, rows), d)[1]
        copies["ag", layer, d] = (
            send(a, a, Z, z_slot(0, layer, d - 1, 0), z_right),
            send(b, b, Z, z_slot(0, layer, d - 1, 1), z_left),
        )

    def gather_wait(layer, d):
        for copy in copies["ag", layer, d]:
            copy.wait_recv()

    def sum_send(layer, k):
        d = half - k
        a = sides(block((t + d) % T, part), d)[0]
        b = sides(block((t + T - d) % T, part), d)[1]
        to_a = sides(from_left.at[layer * half + k], d)[0]
        to_b = sides(from_right.at[layer * half + k], d)[1]
        copies["rs", layer, k] = (
            send(a, to_a, Z, z_slot(1, layer, k, 0), z_right),
            send(b, to_b, Z, z_slot(1, layer, k, 1), z_left),
        )

    def sum_step(layer, k):
        for copy in copies["rs", layer, k - 1]:
            copy.wait_recv()
        d = half - k
        for way, where, buffer in ((0, (t + d) % T, from_left), (1, (t + T - d) % T, from_right)):
            mine = sides(block(where, part), d + 1)[way]
            came = sides(buffer.at[layer * half + k - 1], d + 1)[way]
            mine[...] = (mine[...].astype(jnp.float32) + came[...].astype(jnp.float32)).astype(jnp.bfloat16)
        sum_send(layer, k)

    def sum_own(layer):
        for copy in copies["rs", layer, half - 1]:
            copy.wait_recv()
        own = block(t, part)[...].astype(jnp.float32)
        a = from_left.at[layer * half + half - 1]
        b = from_right.at[layer * half + half - 1]
        if half > 1:
            return own + a[...].astype(jnp.float32) + b[...].astype(jnp.float32)
        came = jnp.concatenate([a[:, :cut], b[:, cut:]], axis=1)
        return own + came.astype(jnp.float32)

    def up(layer):
        gate, value = full[3 * layer], full[3 * layer + 1]
        wide = gate.shape[1]
        tile = 256 if wide % 256 == 0 else 128

        @pl.loop(0, wide // tile)
        def _(j):
            at = pl.ds(pl.multiple_of(j * tile, tile), tile)
            x = all_rows[layer][...]
            a = jnp.dot(x, gate[:, at], preferred_element_type=jnp.float32)
            b = jnp.dot(x, value[:, at], preferred_element_type=jnp.float32)
            hidden[:, at] = (a / (1.0 + jnp.exp(-a)) * b).astype(jnp.bfloat16)

    def down(layer):
        weight = full[3 * layer + 2]
        wide = weight.shape[2]
        tile = 256 if wide % 256 == 0 else 128
        per = wide // tile

        @pl.loop(0, F * per)
        def _(j):
            inside = pl.ds(pl.multiple_of(j % per * tile, tile), tile)
            at = pl.ds(pl.multiple_of(j * tile, tile), tile)
            y = jnp.dot(hidden[...], weight[j // per, :, inside], preferred_element_type=jnp.float32)
            part[:, at] = y.astype(jnp.bfloat16)

    start_weights(0)
    start_weights(1)
    block(t, rows0)[...] = rms_scale(tokens[...].astype(jnp.float32), early_norm[...]).astype(jnp.bfloat16)
    gather_send(0, 1)
    for m in range(2, 6):
        start_weights(m)
    ring_relay(0)
    for d in range(1, half):
        gather_wait(0, d)
        gather_send(0, d + 1)
    ring_relay(1)
    peer_relay(0)
    gather_wait(0, half)
    ring_relay(2)
    peer_relay(1)
    ready(0)
    ready(1)
    up(0)
    ring_relay(3)
    peer_relay(2)
    ready(2)
    down(0)
    sum_send(0, 0)
    for k in range(1, half):
        sum_step(0, k)
    ring_relay(4)
    peer_relay(3)
    branch = sum_own(0)
    keep = (
        tokens[...].astype(jnp.float32)
        + 0.5 * rms_scale(branch, early_post[...])
        + rms_scale(mixer[...].astype(jnp.float32), mixer_gain[...])
    ).astype(jnp.bfloat16)
    mixed[...] = keep
    block(t, rows1)[...] = rms_scale(keep.astype(jnp.float32), later_norm[...]).astype(jnp.bfloat16)
    gather_send(1, 1)
    for k in range(half):
        for copy in copies["rs", 0, k]:
            copy.wait_send()
            done.add(id(copy))
    ring_relay(5)
    peer_relay(4)
    for d in range(1, half):
        gather_wait(1, d)
        gather_send(1, d + 1)
    gather_wait(1, half)
    ready(3)
    ready(4)
    up(1)
    peer_relay(5)
    ready(5)
    down(1)
    sum_send(1, 0)
    for k in range(1, half):
        sum_step(1, k)
    branch = sum_own(1)
    out[...] = (
        mixed[...].astype(jnp.float32) + 0.5 * rms_scale(branch, later_post[...])
    ).astype(jnp.bfloat16)
    for copy in pending:
        if id(copy) not in done:
            copy.wait_send()


def on_device(sizes, *args):
    R, F, T = sizes
    (tokens, mixer, early_norm, eg, ev, ed, early_post, mixer_gain, later_norm, lg, lv, ld, later_post) = args
    n, D = tokens.shape
    depth, wide = eg.shape
    bf16 = jnp.bfloat16
    gains = [x.reshape(1, D) for x in (early_norm, early_post, mixer_gain, later_norm, later_post)]
    vmem = pl.BlockSpec(memory_space=pltpu.VMEM)
    hbm = pl.BlockSpec(memory_space=pl.ANY)
    gathered = [pltpu.VMEM((F * depth, wide), bf16)] * 2 + [pltpu.VMEM((F,) + ed.shape, bf16)]
    G = F // CORES
    w_count = 6 * (1 + (G - 1) * 2 * R)
    z_count = 4 * T
    return pl.pallas_call(
        functools.partial(kernel, R, F, T),
        out_shape=jax.ShapeDtypeStruct((n, D), bf16),
        in_specs=[vmem] * 3 + [hbm] * 3 + [vmem] * 3 + [hbm] * 3 + [vmem],
        out_specs=vmem,
        scratch_shapes=gathered * 2
        + [
            pltpu.VMEM((T * n, D), bf16),
            pltpu.VMEM((T * n, D), bf16),
            pltpu.VMEM((T * n, wide), bf16),
            pltpu.VMEM((T * n, D), bf16),
            pltpu.VMEM((n, D), bf16),
            pltpu.VMEM((T, n, D), bf16),
            pltpu.VMEM((T, n, D), bf16),
            pltpu.SemaphoreType.DMA((w_count,)),
            pltpu.SemaphoreType.DMA((w_count,)),
            pltpu.SemaphoreType.DMA((6,)),
            pltpu.SemaphoreType.DMA((z_count,)),
            pltpu.SemaphoreType.DMA((z_count,)),
        ],
        compiler_params=pltpu.CompilerParams(
            collective_id=0, has_side_effects=True, vmem_limit_bytes=66_000_000
        ),
    )(tokens, mixer, gains[0], eg, ev, ed, gains[1], gains[2], gains[3], lg, lv, ld, gains[4])


def solution(mesh):
    placed = (
        P(("rep", "fs", "tp"), None),
        P(("rep", "fs", "tp"), None),
        P(),
        P("fs", "tp"),
        P("fs", "tp"),
        P("tp", "fs"),
        P(),
        P(),
        P(),
        P("fs", "tp"),
        P("fs", "tp"),
        P("tp", "fs"),
        P(),
    )
    sizes = tuple(mesh.shape[name] for name in ("rep", "fs", "tp"))
    return jax.shard_map(
        functools.partial(on_device, sizes),
        mesh=mesh,
        in_specs=placed,
        out_specs=P(("rep", "fs", "tp"), None),
        check_vma=False,
    )
```

time: 477 us -> 200 us (0.42)
  waiting for transfers between devices: 411 us -> 0 us
  Pallas kernels: 0 us -> 198 us
  matrix products: 40.1 us -> 0 us
  between operations: 13.6 us -> 0.01 us
  other arithmetic: 10.7 us -> 0 us
    all_gather x8 -> x0, waiting for transfers between devices: 321 us -> none  [the longest x4 144 us: gathered(): return lax.all_gather(part, axis, axis=dim, tiled=True)]
    pallas_call x0 -> x1, Pallas kernels: none -> 198 us  [on_device(): pl.pallas_call(functools.partial(kernel, R, F, T), out_shape=jax.ShapeDty...]
    reduce_scatter x2 -> x0, waiting for transfers between devices: 87 us -> none  [own_rows(): lax.psum_scatter(everything.astype(jnp.bfloat16), axis, scatter_dimension...]
    dot_general x4 -> x0, matrix products: 40.1 us -> none  [the longest x2 25 us: row_term(): return jnp.dot(rows, down_block, preferred_element_type=jnp.float32)]
    reduce_sum x5 -> x0, other arithmetic: 5.49 us -> none  [rms_scale(): jnp.mean(values * values, axis=-1, keepdims=True) + epsilon]
    convert_element_type x3 -> x0, other arithmetic: 5.14 us -> none  [the longest x1 2.13 us: on_device(): return layer_out.astype(jnp.bfloat16)]
  transfers between devices with their start and end apart: 10 -> 0, of which waited for: 10 -> 0; matrix products, arithmetic and copies ran while one was open for 4% -> 0% of each run, Pallas kernels for 0% -> 0%
where the time goes in v1:
time: 200 us
  Pallas kernels  198 us (99%)
    pallas_call x1, Pallas kernels, on_device(): pl.pallas_call(functools.partial(kernel, R, F, T), out_shape=jax.ShapeDty...  198 us

profile of v1, /device:TPU:0, one launch (start us, length us, event | category | flops | bytes accessed | tf_op | source)
XLA Modules:
  0.0 199.9 jit_solution(1322359664319060375)
XLA Ops:
  0.0 198.0 %shard_map.127 = bf16[128,2048]{1,0:T(8,128)(2,1)} custom-call(bf16[128,2048]{1,0:T(8,128)(2,1)} %tokens.1, bf16[128,2048]{1,0:T(8,128)(2,1)} %mixer.1, f32[1,2048]{1,0:T(1,128)} %bitcast.5, bf16[512,1280]{1,0:T(8,128)(2,1)} %w0.1, bf16[512,1280]{1,0:T(8,128)(2,1)} %w1.1, bf16[1280,512]{1,0:T(8,128)(2,1)} %w2.1, f32[1,2048]{1,0:T(1,128)} %bitcast.6, ...), custom_call_target="tpu_custom_call" | custom-call | tf_op jit(solution)/shard_map/pallas_call | solution.py:281
  198.0 1.9 copy.15

commit v2 on v1

v2 whole, which is shorter than its diff:
```python
import functools

import jax
import jax.numpy as jnp
from jax import lax
from jax.experimental import pallas as pl
from jax.experimental.pallas import tpu as pltpu
from jax.sharding import PartitionSpec as P

epsilon = 1e-06
CORES = 2


def rms_scale(values, gain):
    scale = lax.rsqrt(jnp.mean(values * values, axis=-1, keepdims=True) + epsilon)
    return values * scale * gain


def kernel(
    R, F, T, B,
    tokens, mixer, early_norm, w0, w1, w2, early_post, mixer_gain, later_norm, w3, w4, w5, later_post,
    out,
    g0, g1, g2, g3, g4, g5, rows0, rows1, hidden, part0, part1, mixed, from_left, from_right, total,
    w_send, w_recv, local_sem, z_send, z_recv,
):
    source = (w0, w1, w2, w3, w4, w5)
    full = (g0, g1, g2, g3, g4, g5)
    all_rows, parts = (rows0, rows1), (part0, part1)
    r, f, t = lax.axis_index("rep"), lax.axis_index("fs"), lax.axis_index("tp")
    G = F // CORES
    g, c = f // CORES, f % CORES
    U = max(1, 4 // G)
    n, D = tokens.shape
    nb = n // B
    mate = {"fs": g * CORES + 1 - c}
    ahead = {"fs": (g + 1) % G * CORES + c}
    behind = {"fs": (g + G - 1) % G * CORES + c}
    z_right, z_left = {"tp": (t + 1) % T}, {"tp": (t + T - 1) % T}
    peers = [{"rep": (r + k) % R} for k in range(1, R)]

    partners = [mate] + peers
    if G > 1:
        partners += [ahead] if G == 2 else [ahead, behind]
    partners += [z_right] if T == 2 else [z_right, z_left]
    barrier = pltpu.get_barrier_semaphore()
    for who in partners:
        pl.semaphore_signal(barrier, inc=1, device_id=who, device_id_type=pl.DeviceIdType.MESH)
    pl.semaphore_wait(barrier, len(partners))

    pending = []

    def send(src, dst, sems, index, who):
        copy = pltpu.make_async_remote_copy(
            src_ref=src, dst_ref=dst, send_sem=sems[0].at[index], recv_sem=sems[1].at[index],
            device_id=who, device_id_type=pl.DeviceIdType.MESH,
        )
        copy.start()
        pending.append(copy)
        return copy

    slots = {}

    def w_index(*key):
        return slots.setdefault(key, len(slots))

    copies = {}

    def piece(m, shard, q, u):
        q = q * U + u
        if m % 3 == 2:
            count = full[m].shape[1] // (R * U)
            return full[m].at[shard, pl.ds(pl.multiple_of(q * count, count), count)]
        depth = source[m].shape[0]
        count = depth // (R * U)
        return full[m].at[pl.ds(pl.multiple_of(shard * depth + q * count, count), count)]

    def whole_shard(m, shard):
        if m % 3 == 2:
            return full[m].at[shard]
        depth = source[m].shape[0]
        return full[m].at[pl.ds(pl.multiple_of(shard * depth, depth), depth)]

    W = (w_send, w_recv)

    def w_send_to(key, src, dst, who):
        copies[key] = send(src, dst, W, w_index(*key), who)

    def start_weights(m):
        if G > 1:
            count = source[m].shape[0] // (R * U)
            for u in range(U):
                own = source[m].at[pl.ds(pl.multiple_of((r * U + u) * count, count), count)]
                w_send_to(("ring", m, u, 1), own, piece(m, f, r, u), ahead)
        w_send_to(("own", m), source[m], whole_shard(m, f), mate)
        local = pltpu.make_async_copy(source[m], whole_shard(m, f), local_sem.at[m])
        local.start()
        copies["local", m] = local

    def ring_relay(m, u):
        for s in range(1, G):
            copies["ring", m, u, s].wait_recv()
            got = piece(m, (g + G - s) % G * CORES + c, r, u)
            if s < G - 1:
                w_send_to(("ring", m, u, s + 1), got, got, ahead)
            for k, who in enumerate(peers):
                w_send_to(("peer", m, u, s, k), got, got, who)
            w_send_to(("mate", m, u, s), got, got, mate)

    def peer_relay(m, u):
        for s in range(1, G):
            for k in range(len(peers)):
                copies["peer", m, u, s, k].wait_recv()
                got = piece(m, (g + G - s) % G * CORES + c, (r + R - 1 - k) % R, u)
                w_send_to(("pass", m, u, s, k), got, got, mate)

    todo = [("y", 0, u) for u in range(min(1, U))]
    for i in range(1, 6 * U):
        todo += [("y", i // U, i % U), ("x", (i - 1) // U, (i - 1) % U)]
    todo.append(("x", 5, U - 1))

    def relay(upto):
        while todo and upto in todo:
            kind, m, u = todo.pop(0)
            (ring_relay if kind == "y" else peer_relay)(m, u)

    def ready(m):
        copies["local", m].wait()
        copies["own", m].wait_recv()
        for u in range(U):
            for s in range(1, G):
                copies["mate", m, u, s].wait_recv()
                for k in range(len(peers)):
                    copies["pass", m, u, s, k].wait_recv()

    sent = []

    def z_copy(src, dst, kind, layer, b, step, way):
        index = (((kind * 2 + layer) * B + b) * T + step) * 2 + way
        return pltpu.make_async_remote_copy(
            src_ref=src, dst_ref=dst, send_sem=z_send.at[index], recv_sem=z_recv.at[index],
            device_id=(z_right, z_left)[way], device_id_type=pl.DeviceIdType.MESH,
        )

    def z_start(when, copy):
        pl.when(when)(copy.start)
        sent.append((when, copy))

    def batch(b, where):
        return pl.ds(pl.multiple_of((b * T + where) * nb, nb), nb)

    def own_rows(b):
        return pl.ds(b * nb, nb)

    def gather_copy(layer, b, d, way):
        where = (t + T - (d - 1)) % T if way == 0 else (t + d - 1) % T
        rows = all_rows[layer].at[batch(b, where)]
        return z_copy(rows, rows, 0, layer, b, d, way)

    def gather_send(layer, b, d):
        z_start((t >= d - 1) & (t < T - 1), gather_copy(layer, b, d, 0))
        z_start((T - 1 - t >= d - 1) & (t > 0), gather_copy(layer, b, d, 1))

    def gather_wait(layer, b, d):
        pl.when(t >= d)(gather_copy(layer, b, d, 0).wait_recv)
        pl.when(T - 1 - t >= d)(gather_copy(layer, b, d, 1).wait_recv)

    def gather_step(layer, b, d):
        gather_wait(layer, b, d)
        if d < T - 1:
            gather_send(layer, b, d + 1)

    def came(layer, b, where, way):
        return (from_left, from_right)[way].at[(layer * B + b) * T + where]

    def sum_copy(layer, b, where, way):
        return z_copy(parts[layer].at[batch(b, where)], came(layer, b, where, way), 1, layer, b, where, way)

    def sum_first(layer, b):
        for i in range(T - 1):
            for way, where in ((0, T - 1 - i), (1, i)):
                z_start(t == (0, T - 1)[way], sum_copy(layer, b, where, way))

    def sum_step(layer, b, i):
        low = t < T // 2
        for way, where, side in ((0, T - 1 - i, low), (1, i, t >= 0), (0, T - 1 - i, ~low)):
            copy = sum_copy(layer, b, where, way)
            middle = side & ((t > 0) & (t < where) if way == 0 else (t < T - 1) & (t > where))
            last = side & (t == where) & ((t > 0) if way == 0 else (t < T - 1))

            @pl.when(middle)
            def _():
                copy.wait_recv()
                mine = parts[layer].at[batch(b, where)]
                mine[...] = (
                    mine[...].astype(jnp.float32) + came(layer, b, where, way)[...].astype(jnp.float32)
                ).astype(jnp.bfloat16)
                copy.start()

            sent.append((middle, copy))
            pl.when(last)(copy.wait_recv)

    def sum_own(layer, b):
        total[...] = parts[layer][batch(b, t)].astype(jnp.float32)
        for way, here in ((0, t > 0), (1, t < T - 1)):

            @pl.when(here)
            def _():
                total[...] += came(layer, b, t, way)[...].astype(jnp.float32)

        return total[...]

    def up(layer, b):
        gate, value = full[3 * layer], full[3 * layer + 1]
        wide = gate.shape[1]
        tile = 256 if wide % 256 == 0 else 128
        rows = pl.ds(b * T * nb, T * nb)

        @pl.loop(0, wide // tile)
        def _(j):
            at = pl.ds(pl.multiple_of(j * tile, tile), tile)
            x = all_rows[layer][rows]
            p = jnp.dot(x, gate[:, at], preferred_element_type=jnp.float32)
            v = jnp.dot(x, value[:, at], preferred_element_type=jnp.float32)
            hidden[rows, at] = (p / (1.0 + jnp.exp(-p)) * v).astype(jnp.bfloat16)

    def down(layer, b):
        weight = full[3 * layer + 2]
        wide = weight.shape[2]
        tile = 256 if wide % 256 == 0 else 128
        per = wide // tile
        rows = pl.ds(b * T * nb, T * nb)

        @pl.loop(0, F * per)
        def _(j):
            inside = pl.ds(pl.multiple_of(j % per * tile, tile), tile)
            at = pl.ds(pl.multiple_of(j * tile, tile), tile)
            y = jnp.dot(hidden[rows], weight[j // per, :, inside], preferred_element_type=jnp.float32)
            parts[layer][rows, at] = y.astype(jnp.bfloat16)

    def enter(b):
        x = tokens[own_rows(b)].astype(jnp.float32)
        rows0[batch(b, t)] = rms_scale(x, early_norm[...]).astype(jnp.bfloat16)
        gather_send(0, b, 1)

    def middle(b):
        keep = (
            tokens[own_rows(b)].astype(jnp.float32)
            + 0.5 * rms_scale(sum_own(0, b), early_post[...])
            + rms_scale(mixer[own_rows(b)].astype(jnp.float32), mixer_gain[...])
        ).astype(jnp.bfloat16)
        mixed[own_rows(b)] = keep
        rows1[batch(b, t)] = rms_scale(keep.astype(jnp.float32), later_norm[...]).astype(jnp.bfloat16)
        gather_send(1, b, 1)

    def leave(b):
        out[own_rows(b)] = (
            mixed[own_rows(b)].astype(jnp.float32) + 0.5 * rms_scale(sum_own(1, b), later_post[...])
        ).astype(jnp.bfloat16)

    first, last = 0, U - 1
    start_weights(0)
    start_weights(1)
    enter(0)
    for m in range(2, 6):
        start_weights(m)
    for b in range(1, B):
        enter(b)
    for b in range(B):
        for d in range(1, T):
            if d == 2:
                relay(("y", b, first))
            gather_step(0, b, d)
    relay(("y", 2, first))
    relay(("x", 1, last))
    ready(0)
    ready(1)
    up(0, 0)
    relay(("y", 2, last))
    for b in range(1, B):
        up(0, b)
    relay(("x", 2, last))
    ready(2)
    for b in range(B):
        down(0, b)
        sum_first(0, b)
    for i in range(T - 1):
        sum_step(0, 0, i)
        relay(("x", 3, (first, last)[i > 0]))
    middle(0)
    for b in range(1, B):
        for i in range(T - 1):
            sum_step(0, b, i)
            gather_step(1, b - 1, i + 1)
            relay((("y", 4, last), ("x", 4, first), ("y", 5, first))[min(i, 2)])
        middle(b)
        if b == 1:
            relay(("x", 4, last))
            ready(3)
            ready(4)
        up(1, b - 1)
        if b == 1:
            relay(("y", 5, last))
            relay(("x", 5, last))
            ready(5)
        down(1, b - 1)
        sum_first(1, b - 1)
    for d in range(1, T):
        gather_step(1, B - 1, d)
    if B == 1:
        relay(("x", 5, last))
        for m in (3, 4, 5):
            ready(m)
    up(1, B - 1)
    down(1, B - 1)
    sum_first(1, B - 1)
    for b in range(B):
        for i in range(T - 1):
            sum_step(1, b, i)
        leave(b)
    for when, copy in sent:
        pl.when(when)(copy.wait_send)
    for copy in pending:
        copy.wait_send()


def on_device(sizes, *args):
    R, F, T = sizes
    (tokens, mixer, early_norm, eg, ev, ed, early_post, mixer_gain, later_norm, lg, lv, ld, later_post) = args
    n, D = tokens.shape
    depth, wide = eg.shape
    bf16 = jnp.bfloat16
    gains = [x.reshape(1, D) for x in (early_norm, early_post, mixer_gain, later_norm, later_post)]
    vmem = pl.BlockSpec(memory_space=pltpu.VMEM)
    hbm = pl.BlockSpec(memory_space=pl.ANY)
    gathered = [pltpu.VMEM((F * depth, wide), bf16)] * 2 + [pltpu.VMEM((F,) + ed.shape, bf16)]
    G = F // CORES
    U = max(1, 4 // G)
    B = 2
    w_count = 6 * (1 + U * (G - 1) * 2 * R)
    z_count = 8 * B * T
    return pl.pallas_call(
        functools.partial(kernel, R, F, T, B),
        out_shape=jax.ShapeDtypeStruct((n, D), bf16),
        in_specs=[vmem] * 3 + [hbm] * 3 + [vmem] * 3 + [hbm] * 3 + [vmem],
        out_specs=vmem,
        scratch_shapes=gathered * 2
        + [
            pltpu.VMEM((T * n, D), bf16),
            pltpu.VMEM((T * n, D), bf16),
            pltpu.VMEM((T * n, wide), bf16),
            pltpu.VMEM((T * n, D), bf16),
            pltpu.VMEM((T * n, D), bf16),
            pltpu.VMEM((n, D), bf16),
            pltpu.VMEM((2 * B * T, n // B, D), bf16),
            pltpu.VMEM((2 * B * T, n // B, D), bf16),
            pltpu.VMEM((n // B, D), jnp.float32),
            pltpu.SemaphoreType.DMA((w_count,)),
            pltpu.SemaphoreType.DMA((w_count,)),
            pltpu.SemaphoreType.DMA((6,)),
            pltpu.SemaphoreType.DMA((z_count,)),
            pltpu.SemaphoreType.DMA((z_count,)),
        ],
        compiler_params=pltpu.CompilerParams(
            collective_id=0, has_side_effects=True, vmem_limit_bytes=66_000_000
        ),
    )(tokens, mixer, gains[0], eg, ev, ed, gains[1], gains[2], gains[3], lg, lv, ld, gains[4])


def solution(mesh):
    placed = (
        P(("rep", "fs", "tp"), None),
        P(("rep", "fs", "tp"), None),
        P(),
        P("fs", "tp"),
        P("fs", "tp"),
        P("tp", "fs"),
        P(),
        P(),
        P(),
        P("fs", "tp"),
        P("fs", "tp"),
        P("tp", "fs"),
        P(),
    )
    sizes = tuple(mesh.shape[name] for name in ("rep", "fs", "tp"))
    return jax.shard_map(
        functools.partial(on_device, sizes),
        mesh=mesh,
        in_specs=placed,
        out_specs=P(("rep", "fs", "tp"), None),
        check_vma=False,
    )
```

time: 200 us -> 192 us (0.960)
  Pallas kernels: 198 us -> 190 us
    pallas_call x1, Pallas kernels: 198 us -> 190 us  [on_device(): pl.pallas_call(functools.partial(kernel, R, F, T, B), out_shape=jax.Shape...]
where the time goes in v2:
time: 192 us
  Pallas kernels  190 us (99%)
    pallas_call x1, Pallas kernels, on_device(): pl.pallas_call(functools.partial(kernel, R, F, T, B), out_shape=jax.Shape...  190 us

profile of v2, /device:TPU:0, one launch (start us, length us, event | category | flops | bytes accessed | tf_op | source)
XLA Modules:
  0.0 192.0 jit_solution(16391314973522006647)
XLA Ops:
  0.0 190.1 %shard_map.127 = bf16[128,2048]{1,0:T(8,128)(2,1)} custom-call(bf16[128,2048]{1,0:T(8,128)(2,1)} %tokens.1, bf16[128,2048]{1,0:T(8,128)(2,1)} %mixer.1, f32[1,2048]{1,0:T(1,128)} %bitcast.5, bf16[512,1280]{1,0:T(8,128)(2,1)} %w0.1, bf16[512,1280]{1,0:T(8,128)(2,1)} %w1.1, bf16[1280,512]{1,0:T(8,128)(2,1)} %w2.1, f32[1,2048]{1,0:T(1,128)} %bitcast.6, ...), custom_call_target="tpu_custom_call" | custom-call | tf_op jit(solution)/shard_map/pallas_call | solution.py:341
  190.1 1.9 copy.15
